TPU v7x, 32 devices: a whole 2x2x4 slice. The times are simulated.
32 devices in a mesh: ep: 8 (over z, y), tp: 4 (over x, core).
Axes of the slice: x: 2, y: 2, z: 4, core: 2. Of those that a mesh axis runs over, the one named last changes fastest.
Arguments:
- cell_query_rows: bfloat16 [2048, 2048], P('ep', 'tp'), may hold values from -6 to 6
- cell_key_rows: bfloat16 [2048, 2048], P('ep', 'tp'), may hold values from -6 to 6
- cell_value_rows: bfloat16 [2048, 2048], P('ep', 'tp'), may hold values from -6 to 6
- output_gate_logits: bfloat16 [2048, 2048], P('ep', 'tp'), may hold values from -8 to 8
- log_input_gate: float32 [8, 2048], P('tp', 'ep'), may hold values from -4 to 110
- forget_gate_logits: float32 [8, 2048], P('tp', 'ep'), may hold values from -1 to 25
- extra_log_forget: float32 [8, 2048], P('tp', 'ep'), may hold values from -0.7 to 0
- cell_output_scale: float32 [2048], P('tp'), may hold values from 0.1 to 1.9
- tokens_into_experts: bfloat16 [4096, 2048], P(('ep', 'tp')), may hold values from -6 to 6
- expert_norm_scale: float32 [2048], replicated, may hold values from 0.1 to 1.9
- token_expert_index: int32 [4096, 2], P(('ep', 'tp')), may hold values from 0 to 7, all different within a row; in each aligned block of 128 rows (0 to 127, 128 to 255, ...) at most 40 rows name the same one
- chosen_expert_weight: float32 [4096, 2], P(('ep', 'tp')), may hold values from 0.3 to 3
- expert_gate_weight: bfloat16 [8, 2048, 3584], P('ep', None, 'tp'), may hold values from -0.125 to 0.125
- expert_up_weight: bfloat16 [8, 2048, 3584], P('ep', None, 'tp'), may hold values from -0.125 to 0.125
- expert_down_weight: bfloat16 [8, 3584, 2048], P('ep', 'tp'), may hold values from -0.09375 to 0.09375
Outputs:
- gated_head_output: bfloat16 [2048, 2048], P('ep', 'tp')
- expert_output: bfloat16 [4096, 2048], P(('ep', 'tp'))
Inputs may be any that keep to these rules, and one draw needn't show every extreme that they name: `token_expert_index`: each row names 2 different experts. Among the rows of one device (aligned blocks of 128 rows) no expert is named by more than 40 rows, and in every draw some expert is named by exactly 40 rows of some device.
All inputs are finite; a program needn't handle non-finite values.
Results may differ from a plain program's by a relative error of at most 0.012.
Values may be sent and summed in bfloat16 or wider, within the bound.
A program may use at most 128 MiB of HBM per device.

v0:
```python
import jax
import jax.numpy as jnp
from jax import lax
from jax.sharding import PartitionSpec as P

HEAD_DIM = 256
BLOCK = 64
TOPK = 2
EPSILON = 1e-06
PRECISE = lax.Precision.HIGHEST


def carried_in(x, axis, combine, identity):
    size, here = (lax.axis_size(axis), lax.axis_index(axis))
    everything = jax.tree.map(lambda part: lax.all_gather(part, axis), x)
    start = jax.tree.map(
        lambda part, zero: jnp.broadcast_to(jnp.asarray(zero, part.dtype), part.shape), x, identity
    )

    def step(k, before):
        reached = k < here
        new = combine(before, jax.tree.map(lambda part: part[k], everything))
        return jax.tree.map(lambda a, b: jnp.where(reached, a, b), new, before)

    return lax.fori_loop(0, size, step, start)


def combine(earlier, later):
    cell_early, norm_early, stab_early, total_early = earlier
    cell_late, norm_late, stab_late, total_late = later
    stabilizer = jnp.maximum(total_late + stab_early, stab_late)
    keep_factor = jnp.exp(total_late + stab_early - stabilizer)
    take_factor = jnp.exp(stab_late - stabilizer)
    cell_state = (
        keep_factor[..., None, None] * cell_early + take_factor[..., None, None] * cell_late
    )
    norm_state = keep_factor[..., None] * norm_early + take_factor[..., None] * norm_late
    return (cell_state, norm_state, stabilizer, total_early + total_late)


def mix_heads(
    cell_query_rows,
    cell_key_rows,
    cell_value_rows,
    output_gate_logits,
    log_input_gate,
    forget_gate_logits,
    extra_log_forget,
    cell_output_scale,
):
    n_tok, row_width = cell_query_rows.shape
    head_count = row_width // HEAD_DIM
    block_count = n_tok // BLOCK
    key_scale = HEAD_DIM ** (-0.5)
    block_shape = (block_count, BLOCK, head_count, HEAD_DIM)
    query_blocks = cell_query_rows.reshape(block_shape)
    key_blocks = cell_key_rows.reshape(block_shape)
    value_blocks = cell_value_rows.reshape(block_shape)
    gate_input = log_input_gate.reshape(head_count, block_count, BLOCK)
    forget_gate_value = (jax.nn.log_sigmoid(forget_gate_logits) + extra_log_forget).reshape(
        head_count, block_count, BLOCK
    )
    cumulative = jnp.cumsum(forget_gate_value, axis=-1)
    block_last = cumulative[..., -1]
    growth = block_last[..., None] - cumulative + gate_input
    block_top = jnp.max(growth, axis=-1)
    shares = jnp.exp(growth - block_top[..., None])
    key_float = key_blocks.astype(jnp.float32) * key_scale
    value_weighted = value_blocks.astype(jnp.float32) * shares.transpose(1, 2, 0)[..., None]
    cell_terms = jnp.einsum("bshv,bshk->bhvk", value_weighted, key_float, precision=PRECISE)
    norm_terms = jnp.einsum("hbs,bshk->bhk", shares, key_float, precision=PRECISE)
    block_terms = (cell_terms, norm_terms, block_top.T, block_last.T)
    identity_state = (
        jnp.zeros((head_count, HEAD_DIM, HEAD_DIM), jnp.float32),
        jnp.zeros((head_count, HEAD_DIM), jnp.float32),
        jnp.full((head_count,), -1e30, jnp.float32),
        jnp.zeros((head_count,), jnp.float32),
    )

    def fold_step(running, block_term):
        return (combine(running, block_term), running)

    device_total, before = lax.scan(fold_step, identity_state, block_terms)
    prior_state = carried_in(device_total, "ep", combine, identity_state)
    zero_state = (
        jnp.zeros((head_count, HEAD_DIM, HEAD_DIM), jnp.float32),
        jnp.zeros((head_count, HEAD_DIM), jnp.float32),
        jnp.zeros((head_count,), jnp.float32),
        jnp.zeros((head_count,), jnp.float32),
    )
    start_state = combine(zero_state, prior_state)
    cell_state, norm_state, stabilizer, _ = combine(start_state, before)
    inter_log = cumulative + stabilizer.T[:, :, None]
    causal = jnp.tril(jnp.ones((BLOCK, BLOCK), dtype=bool))
    spread = jnp.where(
        causal,
        cumulative[..., :, None] - cumulative[..., None, :] + gate_input[..., None, :],
        -jnp.inf,
    )
    row_top = jnp.maximum(inter_log, jnp.max(spread, axis=-1))
    intra_weight = jnp.exp(spread - row_top[..., None])
    inter_weight = jnp.exp(inter_log - row_top)
    scores = (
        jnp.einsum("bthd,bshd->hbts", query_blocks, key_blocks, preferred_element_type=jnp.float32)
        * key_scale
        * intra_weight
    )
    weights = scores.astype(jnp.bfloat16)
    numerator = jnp.einsum(
        "hbts,bshd->hbtd", weights, value_blocks, preferred_element_type=jnp.float32
    )
    query_float = query_blocks.astype(jnp.float32)
    numerator = numerator + inter_weight[..., None] * jnp.einsum(
        "bhvk,bthk->hbtv", cell_state, query_float, precision=PRECISE
    )
    denominator = jnp.sum(scores, axis=-1) + inter_weight * jnp.einsum(
        "bhk,bthk->hbt", norm_state, query_float, precision=PRECISE
    )
    cell_out = numerator / jnp.maximum(jnp.abs(denominator), 1.0)[..., None]
    cell_out = cell_out.transpose(1, 2, 0, 3).reshape(n_tok, row_width)
    return (
        cell_out * cell_output_scale * jax.nn.sigmoid(output_gate_logits.astype(jnp.float32))
    ).astype(jnp.bfloat16)


def slot_tables(ids, experts, capacity):
    flat_ids = ids.reshape(-1)
    onehot = (flat_ids[:, None] == jnp.arange(experts, dtype=jnp.int32)[None, :]).astype(jnp.int32)
    earlier = jnp.cumsum(onehot, axis=0) - onehot
    rank_in = jnp.sum(earlier * onehot, axis=1)
    slot_index = flat_ids * capacity + rank_in
    token_of = jnp.arange(flat_ids.shape[0], dtype=jnp.int32) // ids.shape[1]
    slot_hit = slot_index[:, None] == jnp.arange(experts * capacity, dtype=jnp.int32)[None, :]
    slot_owner = jnp.sum(jnp.where(slot_hit, token_of[:, None] + 1, 0), axis=0)
    return (slot_owner, slot_index.reshape(ids.shape))


def local(
    cell_query_rows,
    cell_key_rows,
    cell_value_rows,
    output_gate_logits,
    log_input_gate,
    forget_gate_logits,
    extra_log_forget,
    cell_output_scale,
    tokens_into_experts,
    expert_norm_scale,
    token_expert_index,
    chosen_expert_weight,
    expert_gate_weight,
    expert_up_weight,
    expert_down_weight,
):
    gated_head_output = mix_heads(
        cell_query_rows,
        cell_key_rows,
        cell_value_rows,
        output_gate_logits,
        log_input_gate,
        forget_gate_logits,
        extra_log_forget,
        cell_output_scale,
    )
    ep_count = lax.axis_size("ep")
    n_tok = tokens_into_experts.shape[0]
    experts = ep_count * expert_gate_weight.shape[0]
    capacity = n_tok * TOPK * 5 // (4 * experts)
    input_float = tokens_into_experts.astype(jnp.float32)
    normed = (
        input_float
        * lax.rsqrt(jnp.mean(input_float * input_float, axis=-1, keepdims=True) + EPSILON)
        * expert_norm_scale
    ).astype(jnp.bfloat16)
    gate_matrix = expert_gate_weight[0]
    up_matrix = expert_up_weight[0]
    down_matrix = expert_down_weight[0]
    slot_owner, slot_index = slot_tables(token_expert_index, experts, capacity)
    sendbuf = jnp.where(
        (slot_owner > 0)[:, None],
        normed[jnp.maximum(slot_owner - 1, 0)],
        jnp.zeros((), jnp.bfloat16),
    )
    arrived = lax.all_to_all(sendbuf, "ep", split_axis=0, concat_axis=0, tiled=True)
    routed_rows = lax.all_gather(arrived, "tp", axis=0, tiled=True)
    gate_out = jnp.dot(routed_rows, gate_matrix, preferred_element_type=jnp.float32)
    up_out = jnp.dot(routed_rows, up_matrix, preferred_element_type=jnp.float32)
    hidden = (jax.nn.silu(gate_out) * up_out).astype(jnp.bfloat16)
    summed = lax.psum_scatter(
        jnp.dot(hidden, down_matrix, preferred_element_type=jnp.float32).astype(jnp.bfloat16),
        "tp",
        scatter_dimension=0,
        tiled=True,
    )
    returned = lax.all_to_all(summed, "ep", split_axis=0, concat_axis=0, tiled=True)
    picked = returned[slot_index]
    expert_output = jnp.sum(
        chosen_expert_weight[..., None] * picked.astype(jnp.float32), axis=1
    ).astype(jnp.bfloat16)
    return (gated_head_output, expert_output)


def solution(mesh):
    return jax.shard_map(
        local,
        mesh=mesh,
        in_specs=(
            P("ep", "tp"),
            P("ep", "tp"),
            P("ep", "tp"),
            P("ep", "tp"),
            P("tp", "ep"),
            P("tp", "ep"),
            P("tp", "ep"),
            P("tp"),
            P(("ep", "tp"), None),
            P(),
            P(("ep", "tp"), None),
            P(("ep", "tp"), None),
            P("ep", None, "tp"),
            P("ep", None, "tp"),
            P("ep", "tp", None),
        ),
        out_specs=(P("ep", "tp"), P(("ep", "tp"), None)),
        check_vma=False,
    )
```

profile of v0, /device:TPU:0, one launch (start us, length us, event | category | flops | bytes accessed | tf_op | source)
XLA Modules:
  0.0 271.6 jit_solution(12901544852267951957)
XLA Ops:
  7.2 0.8 copy.103
  8.3 0.6 reduce-window.6
  8.9 0.2 slice_reduce_fusion
  9.4 1.2 fusion.31
  10.8 1.2 fusion.33
  12.0 2.4 gather_fusion
  14.7 38.7 %all_to_all.21 = bf16[8,40,2048]{2,1,0:T(8,128)(2,1)} all-to-all(bf16[8,40,2048]{2,1,0:T(8,128)(2,1)S(1)} %broadcast_select_fusion.7), channel_id=1, replica_groups=mesh['ep'=8,'tp'=4] {'ep'}, dimensions={0} | all-to-all | bytes 2621440 | tf_op jit(solution)/shard_map/all_to_all | solution.py:184
  53.8 0.5 reduce_window_sum.28
  54.8 0.4 fusion.34
  55.4 2.0 fusion.35
  57.4 4.8 %while.45 = (s32[]{:T(128)}, f32[2,256,256]{2,1,0:T(8,128)S(1)}, f32[2,256]{1,0:T(2,128)S(1)}, f32[2]{0:T(128)S(1)}, f32[2]{0:T(128)S(1)}, /*index=5*/f32[4,2,25...) while((s32[]{:T(128)}, f32[2,256,256]{2,1,0:T(8,128)S(1)}, ...), condition=%wide.region_3.4_spmd.clone, body=%wide.region_2.3_spmd.clone.sunk | while | flops 657939 | bytes 2632544 | solution.py:83
  57.5 0.8 bitcast_dynamic-update-slice_fusion.4
  58.6 0.8 bitcast_dynamic-update-slice_fusion.4
  59.8 0.8 bitcast_dynamic-update-slice_fusion.4
  61.0 0.8 bitcast_dynamic-update-slice_fusion.4
  62.2 0.8 copy-done
  63.0 30.0 %all-gather.8.cloned.1.call-done = bf16[1280,2048]{1,0:T(8,128)(2,1)} async-done(((bf16[320,2048]{1,0:T(8,128)(2,1)}), bf16[1280,2048]{1,0:T(8,128)(2,1)}) %all-gather.8.cloned.1.call-update) | async-done | bytes 5242896 | tf_op jit(solution)/shard_map/all_gather | solution.py:185
  93.0 10.0 %fusion.18 = f32[1280,896]{1,0:T(8,128)} fusion(bf16[1280,2048]{1,0:T(8,128)(2,1)} %all-gather.8.cloned.1.call-done, bf16[1,2048,896]{2,1,0:T(8,128)(2,1)} %param.31), kind=kOutput, calls=%fused_computation.43 | convolution fusion | flops 4697620480 | bytes 13500416 | tf_op jit(solution)/shard_map/dot_general | solution.py:186
  103.0 17.9 %convolution_convert_fusion = bf16[1280,2048]{1,0:T(8,128)(2,1)} fusion(bf16[1,896,2048]{2,1,0:T(8,128)(2,1)} %param.33, f32[1280,896]{1,0:T(8,128)} %fusion.18, bf16[1280,2048]{1,0:T(8,128)(2,1)} %all-gather.8.cloned.1.call-done, bf16[1,2048,896]{2,1,0:T(8,128)(2,1)} %param.32), kind=kOutput, calls=%fused_computation.39 | convolution fusion | flops 9404743680 | bytes 22413312 | tf_op jit(solution)/shard_map/dot_general | solution.py:190
  120.9 0.6 copy-done.12
  121.5 0.6 dynamic-slice
  122.8 0.2 dynamic-update-slice
  123.0 0.2 dynamic-update-slice.1
  123.2 22.6 %all-reduce.2 = (f32[16]{0:T(128)S(1)}, f32[16]{0:T(128)S(1)}) all-reduce(f32[16]{0:T(128)S(1)} %dynamic-update-slice, f32[16]{0:T(128)S(1)} %dynamic-update-slice.1), channel_id=2, replica_groups=mesh['ep'=8,'tp'=4] {'ep'}, use_global_device_ids=true, to_apply=%add | all-reduce | flops 32 | bytes 256
  146.6 26.9 %all-gather.4 = f32[8,2,256]{2,1,0:T(2,128)S(1)} all-gather(f32[1,2,256]{2,1,0:T(2,128)S(1)} %bitcast.169), channel_id=5, replica_groups=mesh['ep'=8,'tp'=4] {'ep'}, dimensions={0}, use_global_device_ids=true | all-gather | bytes 18432 | tf_op jit(solution)/shard_map/all_gather | solution.py:15
  173.6 0.2 fusion.44
  173.8 11.0 %while.46 = (s32[]{:T(128)}, f32[2,256,256]{2,1,0:T(8,128)S(1)}, f32[2,256]{1,0:T(2,128)S(1)}, f32[2]{0:T(128)S(1)}, f32[2]{0:T(128)S(1)}, /*index=5*/s32[]{:T(1...) while((s32[]{:T(128)}, f32[2,256,256]{2,1,0:T(8,128)S(1)}, ...), condition=%wide.region_5.6_spmd.clone, body=%wide.region_4.5_spmd.clone.sunk | while | flops 657944 | bytes 1579285 | solution.py:25
  173.9 1.2 fusion.92
  175.2 1.3 fusion.92
  176.7 1.2 fusion.92
  178.0 1.3 fusion.92
  179.4 1.3 fusion.92
  180.9 1.2 fusion.92
  182.2 1.2 fusion.92
  183.6 1.2 fusion.92
  184.9 36.8 %reduce-scatter.2.cloned.1.call-done = bf16[320,2048]{1,0:T(8,128)(2,1)} async-done(((bf16[1280,2048]{1,0:T(8,128)(2,1)}), bf16[320,2048]{1,0:T(8,128)(2,1)}) %reduce-scatter.2.cloned.1.call-update) | async-done | bytes 1310736 | tf_op jit(solution)/shard_map/reduce_scatter | solution.py:189
  221.7 5.5 %all-to-all-start.1 = ((bf16[8,40,2048]{2,1,0:T(8,128)(2,1)}), bf16[8,40,2048]{2,1,0:T(8,128)(2,1)S(1)}, u32[]{:S(2)}, u32[]{:S(2)}) async-start(bf16[8,40,2048]{2,1,0:T(8,128)(2,1)} %bitcast.168), calls=%async_computation.2 | async-start | bytes 2621440 | tf_op jit(solution)/shard_map/all_to_all | solution.py:195
  227.6 0.3 fusion.48
  227.9 0.3 fusion.71
  228.4 0.6 copy-done.1
  229.1 1.5 fusion.27
  230.6 0.3 fusion.26
  230.9 0.4 copy.101
  231.5 0.9 multiply_convert_fusion.1
  232.4 26.1 %all-to-all-done.1 = bf16[8,40,2048]{2,1,0:T(8,128)(2,1)S(1)} async-done(((bf16[8,40,2048]{2,1,0:T(8,128)(2,1)}), bf16[8,40,2048]{2,1,0:T(8,128)(2,1)S(1)}, u32[]{:S(2)}, u32[]{:S(2)}) %all-to-all-start.1) | async-done | bytes 1310752 | tf_op jit(solution)/shard_map/all_to_all | solution.py:195
  258.5 1.4 gather_fusion.1
  259.8 1.3 reshape.175
  261.2 3.9 %multiply_reduce_fusion = bf16[128,2048]{1,0:T(8,128)(2,1)} fusion(f32[128,2,2048]{2,1,0:T(2,128)S(1)} %reshape.175, f32[128,2]{1,0:T(8,128)S(1)} %copy.102), kind=kLoop, calls=%fused_computation.47 | loop fusion | flops 786432 | bytes 2622464 | tf_op jit(solution)/shard_map/reduce_sum | solution.py:197
  (149 shorter events, 5.9 us)
Async XLA Ops:
  7.2 85.9 %all-gather.8.cloned.1.call-start = ((), (), s32[]{:S(2)}) async-start(), calls=%async_computation.3 | async-start | bytes 6553600 | tf_op jit(solution)/shard_map/all_gather | solution.py:185
  14.6 38.9 %copy-start.8 = (f32[2,256]{1,0:T(2,128)S(1)}, f32[2,256]{1,0:T(2,128)}, u32[]{:S(2)}) copy-start(f32[2,256]{1,0:T(2,128)} %param.25) | copy-start | bytes 6148
  14.6 38.9 %copy-start.9 = (f32[2,256]{1,0:T(2,128)S(1)}, f32[2,256]{1,0:T(2,128)}, u32[]{:S(2)}) copy-start(f32[2,256]{1,0:T(2,128)} %param.24) | copy-start | bytes 6148
  14.6 39.0 %copy-start.10 = (f32[2,256]{1,0:T(2,128)S(1)}, f32[2,256]{1,0:T(2,128)}, u32[]{:S(2)}) copy-start(f32[2,256]{1,0:T(2,128)} %param.23) | copy-start | bytes 6148
  14.6 40.0 %copy-start.2 = (bf16[256,512]{1,0:T(8,128)(2,1)S(1)}, bf16[256,512]{1,0:T(8,128)(2,1)}, u32[]{:S(2)}) copy-start(bf16[256,512]{1,0:T(8,128)(2,1)} %param.20) | copy-start | bytes 786436
  14.7 40.1 %copy-start.3 = (bf16[256,512]{1,0:T(8,128)(2,1)S(1)}, bf16[256,512]{1,0:T(8,128)(2,1)}, u32[]{:S(2)}) copy-start(bf16[256,512]{1,0:T(8,128)(2,1)} %param.21) | copy-start | bytes 786436
  53.4 120.4 %all-gather.10.cloned.1.call-start = ((), (), s32[]{:S(2)}) async-start(), calls=%async_computation.5 | async-start | bytes 4718592 | tf_op jit(solution)/shard_map/all_gather | solution.py:15
  62.1 0.8 copy-start
  63.0 158.7 %reduce-scatter.2.cloned.1.call-start = ((), (), s32[]{:S(2)}) async-start(), calls=%async_computation.4 | async-start | bytes 6553600 | tf_op jit(solution)/shard_map/reduce_scatter | solution.py:189
  120.9 0.7 copy-start.12
  120.9 25.2 %copy-start.4 = (bf16[256,512]{1,0:T(8,128)(2,1)S(1)}, bf16[256,512]{1,0:T(8,128)(2,1)}, u32[]{:S(2)}) copy-start(bf16[256,512]{1,0:T(8,128)(2,1)} %param.19) | copy-start | bytes 786436
  120.9 25.4 %copy-start.6 = (s32[128,2]{0,1:T(2,128)S(1)}, s32[128,2]{0,1:T(2,128)}, u32[]{:S(2)}) copy-start(s32[128,2]{0,1:T(2,128)} %param.29) | copy-start | bytes 3076
  120.9 25.6 %copy-start.11 = (f32[128,2]{0,1:T(2,128)S(1)}, f32[128,2]{0,1:T(2,128)}, u32[]{:S(2)}) copy-start(f32[128,2]{0,1:T(2,128)} %param.30) | copy-start | bytes 3076
  221.7 36.8 %all-to-all-start.1 = ((bf16[8,40,2048]{2,1,0:T(8,128)(2,1)}), bf16[8,40,2048]{2,1,0:T(8,128)(2,1)S(1)}, u32[]{:S(2)}, u32[]{:S(2)}) async-start(bf16[8,40,2048]{2,1,0:T(8,128)(2,1)} %bitcast.168), calls=%async_computation.2 | async-start | bytes 2621440 | tf_op jit(solution)/shard_map/all_to_all | solution.py:195
  227.5 1.6 copy-start.1
  230.5 1.0 copy-start.5
  230.6 0.9 copy-start.7
Sparse Core Ops, SparseCore 0:
  53.5 39.4 all-gather.7
  95.7 73.2 all-gather.9
  171.5 50.1 reduce-scatter.1
where the time goes:
time: 272 us
  waiting for transfers between devices  93 us (34%)
  blocking collectives  88.2 us (32%)
  matrix products  32.6 us (12%)
  other arithmetic  25 us (9%)
  between operations  14.8 us (5%)
  local copies, waits for them, and re-layouts  12.1 us (4%)
  starting transfers between devices  5.64 us (2%)
    all_to_all x1, blocking collectives, local(): lax.all_to_all(sendbuf, 'ep', split_axis=0, concat_axis=0, tiled=True)  38.7 us
    reduce_scatter x1, waiting for transfers between devices, local(): lax.psum_scatter(jnp.dot(hidden, down_matrix, preferred_element_type=jnp....  36.8 us
    all_gather x1, waiting for transfers between devices, local(): routed_rows = lax.all_gather(arrived, 'tp', axis=0, tiled=True)  30 us
    all_gather x1, blocking collectives, carried_in(): everything = jax.tree.map(lambda part: lax.all_gather(part, axis), x)  26.9 us
    all_to_all x1, waiting for transfers between devices, local(): lax.all_to_all(summed, 'ep', split_axis=0, concat_axis=0, tiled=True)  26.1 us
    unnamed x1, blocking collectives  22.6 us
    dot_general x1, matrix products, local(): jnp.dot(hidden, down_matrix, preferred_element_type=jnp.float32)  17.9 us
    select_n x24, other arithmetic, step(): return jax.tree.map(lambda a, b: jnp.where(reached, a, b), new, before)  10.8 us
  transfers between devices with their start and end apart: 4, of which 3 were waited for; matrix products, arithmetic and copies ran while one was open for 20% of the time, Pallas kernels for 0%

commit v1 on v0

--- a/solution.py
+++ b/solution.py
@@ -182,7 +182,12 @@
         jnp.zeros((), jnp.bfloat16),
     )
     arrived = lax.all_to_all(sendbuf, "ep", split_axis=0, concat_axis=0, tiled=True)
-    routed_rows = lax.all_gather(arrived, "tp", axis=0, tiled=True)
+    ring = [arrived]
+    for hop in range(3):
+        ring.append(lax.ppermute(ring[-1], "tp", [(dev, (dev + 1) % 4) for dev in range(4)]))
+    routed_rows = jnp.roll(
+        jnp.concatenate(ring[::-1], axis=0), (lax.axis_index("tp") + 1) * ring[0].shape[0], axis=0
+    )
     gate_out = jnp.dot(routed_rows, gate_matrix, preferred_element_type=jnp.float32)
     up_out = jnp.dot(routed_rows, up_matrix, preferred_element_type=jnp.float32)
     hidden = (jax.nn.silu(gate_out) * up_out).astype(jnp.bfloat16)

time: 272 us -> 234 us (0.86)
  waiting for transfers between devices: 93 us -> 50.1 us
  local copies, waits for them, and re-layouts: 12.1 us -> 20 us
  matrix products: 32.6 us -> 28.6 us
  other arithmetic: 25 us -> 28.8 us
  blocking collectives: 88.2 us -> 84.6 us
    reduce_scatter x1, waiting for transfers between devices: 36.8 us -> 0.03 us  [local(): lax.psum_scatter(jnp.dot(hidden, down_matrix, preferred_element_type=jnp....]
    ppermute x0 -> x3, waiting for transfers between devices: none -> 32.9 us  [local(): lax.ppermute(ring[-1], 'tp', [(dev, (dev + 1) % 4) for dev in range(4)])]
    all_gather x1 -> x0, waiting for transfers between devices: 30 us -> none  [local(): routed_rows = lax.all_gather(arrived, 'tp', axis=0, tiled=True)]
    dot_general x1, matrix products: 17.9 us -> 7.4 us  [local(): jnp.dot(hidden, down_matrix, preferred_element_type=jnp.float32)]
    all_to_all x1, waiting for transfers between devices: 26.1 us -> 17.1 us  [local(): lax.all_to_all(summed, 'ep', split_axis=0, concat_axis=0, tiled=True)]
    unnamed x36 -> x47, local copies, waits for them, and re-layouts: 4.43 us -> 10.6 us
    dot_general x0 -> x1, matrix products: none -> 5.96 us  [local(): up_out = jnp.dot(routed_rows, up_matrix, preferred_element_type=jnp.float32)]
    dot_general x1, matrix products: 9.98 us -> 5.62 us  [local(): jnp.dot(routed_rows, gate_matrix, preferred_element_type=jnp.float32)]
  transfers between devices with their start and end apart: 4 -> 6, of which waited for: 3 -> 4; matrix products, arithmetic and copies ran while one was open for 20% -> 26% of each run, Pallas kernels for 0% -> 0%
where the time goes in v1:
time: 234 us; the launch traced here: 233 us
  blocking collectives  84.6 us (36%)
  waiting for transfers between devices  50.1 us (21%)
  other arithmetic  28.8 us (12%)
  matrix products  28.6 us (12%)
  local copies, waits for them, and re-layouts  20 us (9%)
  between operations  16.7 us (7%)
  starting transfers between devices  3.89 us (2%)
    all_to_all x1, blocking collectives, local(): lax.all_to_all(sendbuf, 'ep', split_axis=0, concat_axis=0, tiled=True)  38.5 us
    ppermute x3, waiting for transfers between devices, local(): lax.ppermute(ring[-1], 'tp', [(dev, (dev + 1) % 4) for dev in range(4)])  32.9 us
    all_gather x1, blocking collectives, carried_in(): everything = jax.tree.map(lambda part: lax.all_gather(part, axis), x)  26.1 us
    unnamed x1, blocking collectives  20 us
    all_to_all x1, waiting for transfers between devices, local(): lax.all_to_all(summed, 'ep', split_axis=0, concat_axis=0, tiled=True)  17.1 us
    unnamed x47, local copies, waits for them, and re-layouts  10.6 us
    select_n x24, other arithmetic, step(): return jax.tree.map(lambda a, b: jnp.where(reached, a, b), new, before)  10.4 us
    dot_general x1, matrix products, local(): jnp.dot(hidden, down_matrix, preferred_element_type=jnp.float32)  7.4 us
  transfers between devices with their start and end apart: 6, of which 4 were waited for; matrix products, arithmetic and copies ran while one was open for 26% of the time, Pallas kernels for 0%

profile of v1, /device:TPU:0, one launch (start us, length us, event | category | flops | bytes accessed | tf_op | source)
XLA Modules:
  0.0 232.9 jit_solution(9945380960502382720)
XLA Ops:
  8.0 0.8 copy.103
  10.3 1.2 fusion.38
  11.6 1.2 fusion.40
  12.8 2.4 %gather_fusion = bf16[320,2048]{1,0:T(8,128)(2,1)S(1)} fusion(bf16[128,2048]{1,0:T(8,128)(2,1)S(1)} %fusion.40, s32[1024]{0:T(1024)S(1)} %pad_clamp_fusion.1), kind=kCustom, calls=%fused_computation | custom fusion | bytes 2622720 | tf_op jit(solution)/shard_map/gather | solution.py:181
  15.5 38.5 %all_to_all.21 = bf16[8,40,2048]{2,1,0:T(8,128)(2,1)S(1)} all-to-all(bf16[8,40,2048]{2,1,0:T(8,128)(2,1)S(1)} %broadcast_select_fusion.7), channel_id=1, replica_groups=mesh['ep'=8,'tp'=4] {'ep'}, dimensions={0} | all-to-all | bytes 2621440 | tf_op jit(solution)/shard_map/all_to_all | solution.py:184
  55.1 0.8 reshape.146
  55.9 1.0 reshape.148
  56.9 1.3 fusion.41
  58.4 4.3 %fusion.42 = f32[4,2,256,256]{3,2,1,0:T(8,128)} fusion(bf16[4,64,2,256]{3,2,1,0:T(2,128)(2,1)S(1)} %reshape.148, f32[4,64,2]{1,2,0:T(2,128)S(1)} %copy.91, bf16[4,64,2,256]{3,2,1,0:T(2,128)(2,1)} %reshape.146), kind=kOutput, calls=%fused_computation.69 | convolution fusion | flops 403177472 | bytes 2623488 | tf_op jit(solution)/shard_map/bshv,bshk->bhvk/dot_general | solution.py:70
  62.7 8.3 %collective-permute-done = bf16[320,2048]{1,0:T(8,128)(2,1)S(1)} collective-permute-done((bf16[320,2048]{1,0:T(8,128)(2,1)S(1)}, bf16[320,2048]{1,0:T(8,128)(2,1)S(1)}, u32[]{:S(2)}, u32[]{:S(2)}) %collective-permute-start) | collective-permute-done | bytes 1310752 | tf_op jit(solution)/shard_map/ppermute | solution.py:187
  71.0 9.0 %while.45 = (s32[]{:T(128)}, f32[2,256,256]{2,1,0:T(8,128)S(1)}, f32[2,256]{1,0:T(2,128)S(1)}, f32[2]{0:T(128)S(1)}, f32[2]{0:T(128)S(1)}, /*index=5*/f32[4,2,25...) while((s32[]{:T(128)}, f32[2,256,256]{2,1,0:T(8,128)S(1)}, ...), condition=%wide.region_3.4_spmd.clone, body=%wide.region_2.3_spmd.clone.sunk | while | flops 657939 | bytes 2632544 | solution.py:83
  71.1 0.8 bitcast_dynamic-update-slice_fusion.4
  71.9 1.2 fusion.88
  73.3 0.8 bitcast_dynamic-update-slice_fusion.4
  74.1 1.2 fusion.88
  75.5 0.9 bitcast_dynamic-update-slice_fusion.4
  76.4 1.2 fusion.88
  77.8 0.9 bitcast_dynamic-update-slice_fusion.4
  78.6 1.2 fusion.88
  80.0 0.8 copy-done
  80.8 7.3 %collective-permute-done.1 = bf16[320,2048]{1,0:T(8,128)(2,1)} collective-permute-done((bf16[320,2048]{1,0:T(8,128)(2,1)S(1)}, bf16[320,2048]{1,0:T(8,128)(2,1)}, u32[]{:S(2)}, u32[]{:S(2)}) %collective-permute-start.1) | collective-permute-done | bytes 1310752 | tf_op jit(solution)/shard_map/ppermute | solution.py:187
  88.2 17.3 %collective-permute-done.2 = bf16[320,2048]{1,0:T(8,128)(2,1)} collective-permute-done((bf16[320,2048]{1,0:T(8,128)(2,1)}, bf16[320,2048]{1,0:T(8,128)(2,1)}, u32[]{:S(2)}, u32[]{:S(2)}) %collective-permute-start.2) | collective-permute-done | bytes 1310752 | tf_op jit(solution)/shard_map/ppermute | solution.py:187
  105.5 1.4 constant_dynamic-update-slice_fusion.7
  107.0 1.5 constant_dynamic-update-slice_fusion.6
  108.6 1.5 constant_dynamic-update-slice_fusion.3
  110.1 1.6 constant_dynamic-update-slice_fusion.2
  112.5 5.6 %fusion.18 = f32[1280,896]{1,0:T(8,128)S(1)} fusion(bf16[2560,2048]{1,0:T(8,128)(2,1)S(1)} %constant_dynamic-update-slice_fusion, s32[]{:T(128)S(6)} %select_n.116, bf16[1,2048,896]{2,1,0:T(8,128)(2,1)S(1)} %copy-done.11), kind=kOutput, calls=%fused_computation.42 | convolution fusion | flops 4697620480 | bytes 13500420 | tf_op jit(solution)/shard_map/dot_general | solution.py:191
  118.2 6.0 %multiply_convert_fusion = bf16[1280,896]{1,0:T(8,128)(2,1)S(1)} fusion(f32[1280,896]{1,0:T(8,128)S(1)} %fusion.18, bf16[1,2048,896]{2,1,0:T(8,128)(2,1)S(1)} %copy-done.12, bf16[2560,2048]{1,0:T(8,128)(2,1)S(1)} %constant_dynamic-update-slice_fusion, s32[]{:T(128)S(6)} %select_n.116), kind=kOutput, calls=%fused_computation.44 | convolution fusion | flops 4704501760 | bytes 15794180 | tf_op jit(solution)/shard_map/dot_general | solution.py:192
  124.1 7.4 %convolution_convert_fusion = bf16[1280,2048]{1,0:T(8,128)(2,1)} fusion(bf16[1280,896]{1,0:T(8,128)(2,1)S(1)} %multiply_convert_fusion, bf16[1,896,2048]{2,1,0:T(8,128)(2,1)S(1)} %copy-done.13), kind=kOutput, calls=%fused_computation.39 | convolution fusion | flops 4700241920 | bytes 11206656 | tf_op jit(solution)/shard_map/dot_general | solution.py:195
  132.2 0.7 dynamic-slice
  134.0 20.0 %all-reduce.2 = (f32[16]{0:T(128)S(1)}, f32[16]{0:T(128)S(1)}) all-reduce(f32[16]{0:T(128)S(1)} %dynamic-update-slice, f32[16]{0:T(128)S(1)} %dynamic-update-slice.1), channel_id=2, replica_groups=mesh['ep'=8,'tp'=4] {'ep'}, use_global_device_ids=true, to_apply=%add | all-reduce | flops 32 | bytes 256
  154.9 26.1 %all-gather.4 = f32[8,2,256]{2,1,0:T(2,128)S(1)} all-gather(f32[1,2,256]{2,1,0:T(2,128)S(1)} %bitcast.163), channel_id=5, replica_groups=mesh['ep'=8,'tp'=4] {'ep'}, dimensions={0}, use_global_device_ids=true | all-gather | bytes 18432 | tf_op jit(solution)/shard_map/all_gather | solution.py:15
  181.3 10.6 %while.46 = (s32[]{:T(128)}, f32[2,256,256]{2,1,0:T(8,128)S(1)}, f32[2,256]{1,0:T(2,128)S(1)}, f32[2]{0:T(128)S(1)}, f32[2]{0:T(128)S(1)}, /*index=5*/s32[]{:T(1...) while((s32[]{:T(128)}, f32[2,256,256]{2,1,0:T(8,128)S(1)}, ...), condition=%wide.region_5.6_spmd.clone, body=%wide.region_4.5_spmd.clone.sunk | while | flops 657944 | bytes 1579285 | solution.py:25
  181.3 1.2 fusion.91
  182.7 1.2 fusion.91
  184.0 1.2 fusion.91
  185.3 1.2 fusion.91
  186.6 1.2 fusion.91
  187.9 1.2 fusion.91
  189.3 1.2 fusion.91
  190.6 1.2 fusion.91
  191.9 3.8 %all-to-all-start.1 = ((bf16[8,40,2048]{2,1,0:T(8,128)(2,1)}), bf16[8,40,2048]{2,1,0:T(8,128)(2,1)S(1)}, u32[]{:S(2)}, u32[]{:S(2)}) async-start(bf16[8,40,2048]{2,1,0:T(8,128)(2,1)} %bitcast.162), calls=%async_computation.2 | async-start | bytes 2621440 | tf_op jit(solution)/shard_map/all_to_all | solution.py:200
  197.0 3.1 %fusion.34 = f32[4,64,2,256]{3,1,0,2:T(8,128)S(1)} fusion(f32[4,64,2]{1,0,2:T(4,128)S(1)} %get-tuple-element.453, bf16[4,64,2,256]{3,2,1,0:T(2,128)(2,1)S(1)} %reshape.145, f32[4,2,256,256]{3,2,1,0:T(8,128)} %get-tuple-element.257, f32[4,2]{1,0:T(4,128)S(1)} %subtract_exponential_fusion.5, f32[2,256,256]{2,1,0:T(8,128)S(1)} %multiply_add_fusion.1, ...), kind=kOutput, calls=%fused_computation.59 | convolution fusion | flops 404357120 | bytes 3409984 | tf_op jit(solution)/shard_map/bhvk,bthk->hbtv/dot_general | solution.py:113
  200.8 0.9 multiply_convert_fusion.1
  201.7 17.1 %all-to-all-done.1 = bf16[8,40,2048]{2,1,0:T(8,128)(2,1)S(1)} async-done(((bf16[8,40,2048]{2,1,0:T(8,128)(2,1)}), bf16[8,40,2048]{2,1,0:T(8,128)(2,1)S(1)}, u32[]{:S(2)}, u32[]{:S(2)}) %all-to-all-start.1) | async-done | bytes 1310752 | tf_op jit(solution)/shard_map/all_to_all | solution.py:200
  218.8 1.4 gather_fusion.1
  220.1 1.3 reshape.175
  221.5 3.9 %multiply_reduce_fusion = bf16[128,2048]{1,0:T(8,128)(2,1)} fusion(f32[128,2,2048]{2,1,0:T(2,128)S(1)} %reshape.175, f32[128,2]{1,0:T(8,128)S(1)} %copy.102), kind=kLoop, calls=%fused_computation.50 | loop fusion | flops 786432 | bytes 2622464 | tf_op jit(solution)/shard_map/reduce_sum | solution.py:202
  (165 shorter events, 9.9 us)
Async XLA Ops:
  8.0 173.2 %all-gather.7.cloned.1.call-start = ((), (), s32[]{:S(2)}) async-start(), calls=%async_computation.4 | async-start | bytes 4718592 | tf_op jit(solution)/shard_map/all_gather | solution.py:15
  15.3 38.7 %copy-start.7 = (f32[2,256]{1,0:T(2,128)S(1)}, f32[2,256]{1,0:T(2,128)}, u32[]{:S(2)}) copy-start(f32[2,256]{1,0:T(2,128)} %param.25) | copy-start | bytes 6148
  15.3 38.7 %copy-start.8 = (f32[2,256]{1,0:T(2,128)S(1)}, f32[2,256]{1,0:T(2,128)}, u32[]{:S(2)}) copy-start(f32[2,256]{1,0:T(2,128)} %param.24) | copy-start | bytes 6148
  15.3 38.8 %copy-start.9 = (f32[2,256]{1,0:T(2,128)S(1)}, f32[2,256]{1,0:T(2,128)}, u32[]{:S(2)}) copy-start(f32[2,256]{1,0:T(2,128)} %param.23) | copy-start | bytes 6148
  15.3 39.8 %copy-start.2 = (bf16[256,512]{1,0:T(8,128)(2,1)S(1)}, bf16[256,512]{1,0:T(8,128)(2,1)}, u32[]{:S(2)}) copy-start(bf16[256,512]{1,0:T(8,128)(2,1)} %param.20) | copy-start | bytes 786436
  54.0 17.0 %collective-permute-start = (bf16[320,2048]{1,0:T(8,128)(2,1)S(1)}, bf16[320,2048]{1,0:T(8,128)(2,1)S(1)}, u32[]{:S(2)}, u32[]{:S(2)}) collective-permute-start(bf16[320,2048]{1,0:T(8,128)(2,1)S(1)} %bitcast.155), channel_id=1, source_target_pairs={{0,1},{1,2},{2,3},{3,0},{4,5},{5,6},{6,7},{7,4},{8,9},{9,10},{10,1... | collective-permute-start | bytes 3932168 | tf_op jit(solution)/shard_map/ppermute | solution.py:187
  71.0 17.1 %collective-permute-start.1 = (bf16[320,2048]{1,0:T(8,128)(2,1)S(1)}, bf16[320,2048]{1,0:T(8,128)(2,1)}, u32[]{:S(2)}, u32[]{:S(2)}) collective-permute-start(bf16[320,2048]{1,0:T(8,128)(2,1)S(1)} %collective-permute-done), channel_id=1, source_target_pairs={{0,1},{1,2},{2,3},{3,0},{4,5},{5,6},{6,7},{7,4},{8,9},{9,10},{10,1... | collective-permute-start | bytes 3932168 | tf_op jit(solution)/shard_map/ppermute | solution.py:187
  80.0 0.8 copy-start
  80.8 111.1 %reduce-scatter.2.cloned.1.call-start = ((), (), s32[]{:S(2)}) async-start(), calls=%async_computation.3 | async-start | bytes 6553600 | tf_op jit(solution)/shard_map/reduce_scatter | solution.py:194
  88.1 17.3 %collective-permute-start.2 = (bf16[320,2048]{1,0:T(8,128)(2,1)}, bf16[320,2048]{1,0:T(8,128)(2,1)}, u32[]{:S(2)}, u32[]{:S(2)}) collective-permute-start(bf16[320,2048]{1,0:T(8,128)(2,1)} %collective-permute-done.1), channel_id=1, source_target_pairs={{0,1},{1,2},{2,3},{3,0},{4,5},{5,6},{6,7},{7,4},{8,9},{9,10},{10,1... | collective-permute-start | bytes 3932168 | tf_op jit(solution)/shard_map/ppermute | solution.py:187
  110.1 2.4 %copy-start.11 = (bf16[1,2048,896]{2,1,0:T(8,128)(2,1)S(1)}, bf16[1,2048,896]{2,1,0:T(8,128)(2,1)}, u32[]{:S(2)}) copy-start(bf16[1,2048,896]{2,1,0:T(8,128)(2,1)} %param.31) | copy-start | bytes 11010052
  112.5 5.6 %copy-start.12 = (bf16[1,2048,896]{2,1,0:T(8,128)(2,1)S(1)}, bf16[1,2048,896]{2,1,0:T(8,128)(2,1)}, u32[]{:S(2)}) copy-start(bf16[1,2048,896]{2,1,0:T(8,128)(2,1)} %param.32) | copy-start | bytes 11010052
  118.1 6.0 %copy-start.13 = (bf16[1,896,2048]{2,1,0:T(8,128)(2,1)S(1)}, bf16[1,896,2048]{2,1,0:T(8,128)(2,1)}, u32[]{:S(2)}) copy-start(bf16[1,896,2048]{2,1,0:T(8,128)(2,1)} %param.33) | copy-start | bytes 11010052
  131.5 0.7 copy-start.14
  131.5 22.7 %copy-start.5 = (s32[128,2]{0,1:T(2,128)S(1)}, s32[128,2]{0,1:T(2,128)}, u32[]{:S(2)}) copy-start(s32[128,2]{0,1:T(2,128)} %param.29) | copy-start | bytes 3076
  131.5 23.0 %copy-start.10 = (f32[128,2]{0,1:T(2,128)S(1)}, f32[128,2]{0,1:T(2,128)}, u32[]{:S(2)}) copy-start(f32[128,2]{0,1:T(2,128)} %param.30) | copy-start | bytes 3076
  131.5 23.2 %copy-start.3 = (bf16[256,512]{1,0:T(8,128)(2,1)S(1)}, bf16[256,512]{1,0:T(8,128)(2,1)}, u32[]{:S(2)}) copy-start(bf16[256,512]{1,0:T(8,128)(2,1)} %param.19) | copy-start | bytes 786436
  181.2 15.2 %copy-start.1 = (bf16[4,64,2,256]{3,2,1,0:T(2,128)(2,1)S(1)}, bf16[4,64,2,256]{3,2,1,0:T(2,128)(2,1)}, u32[]{:S(2)}) copy-start(bf16[4,64,2,256]{3,2,1,0:T(2,128)(2,1)} %reshape.146) | copy-start | bytes 786436
  191.9 26.9 %all-to-all-start.1 = ((bf16[8,40,2048]{2,1,0:T(8,128)(2,1)}), bf16[8,40,2048]{2,1,0:T(8,128)(2,1)S(1)}, u32[]{:S(2)}, u32[]{:S(2)}) async-start(bf16[8,40,2048]{2,1,0:T(8,128)(2,1)} %bitcast.162), calls=%async_computation.2 | async-start | bytes 2621440 | tf_op jit(solution)/shard_map/all_to_all | solution.py:200
  196.9 3.9 %copy-start.4 = (bf16[256,512]{1,0:T(8,128)(2,1)S(1)}, bf16[256,512]{1,0:T(8,128)(2,1)}, u32[]{:S(2)}) copy-start(bf16[256,512]{1,0:T(8,128)(2,1)} %param.22) | copy-start | bytes 786436
  197.0 3.9 %copy-start.6 = (f32[512]{0:T(512)S(1)}, f32[512]{0:T(512)}, u32[]{:S(2)}) copy-start(f32[512]{0:T(512)} %param.26) | copy-start | bytes 6148
Sparse Core Ops, SparseCore 0:
  80.9 72.3 all-gather.6
Sparse Core Ops, SparseCore 1:
  131.7 50.2 reduce-scatter.1
